TPU v7x, 32 devices: a whole 2x2x4 slice. The times are simulated.
32 devices in a mesh: sp: 16 (over z, y, x), tp: 2 (over core).
Axes of the slice: x: 2, y: 2, z: 4, core: 2. Of those that a mesh axis runs over, the one named last changes fastest.
Arguments:
- stream: bfloat16 [7168, 2048], P('sp'), may hold values from -6 to 6
- norm_gain: float32 [2, 2048], replicated, may hold values from 0.1 to 1.9
- value_weight: bfloat16 [2, 2048, 512], P(None, None, 'tp'), may hold values from -0.125 to 0.125
- gate_weight: bfloat16 [2, 2048, 512], P(None, None, 'tp'), may hold values from -0.125 to 0.125
- conv_taps: bfloat16 [2, 512, 512], P(None, None, 'tp'), may hold values from -0.25 to 0.25
- conv_bias: float32 [2, 512], P(None, 'tp'), may hold values from -3 to 3
- channel_gain: float32 [2, 512], replicated, may hold values from 0.1 to 1.9
- channel_shift: float32 [2, 512], replicated, may hold values from -3 to 3
- out_weight: bfloat16 [2, 512, 2048], replicated, may hold values from -0.25 to 0.25
Outputs:
- result: bfloat16 [7168, 2048], P('sp')
All inputs are finite; a program needn't handle non-finite values.
Results may differ from a plain program's by a relative error of at most 0.0075.
Values may be sent and summed in bfloat16 or wider, within the bound.
A program may use at most 64 MiB of HBM per device.

v0:
```python
import jax
import jax.numpy as jnp
from jax import lax
from jax.sharding import PartitionSpec as P


def passed_along(value, axis, by):
    count = lax.axis_size(axis)
    pairs = [(i, i + by) for i in range(count) if 0 <= i + by < count]
    return lax.ppermute(value, axis, pairs)


def rms_normed(stream, gain):
    values = stream.astype(jnp.float32)
    scale = lax.rsqrt(jnp.mean(values * values, axis=-1, keepdims=True) + 1e-06)
    return (values * scale * gain[None, :]).astype(jnp.bfloat16)


def channel_mix(conv, gain, shift):
    values = conv.astype(jnp.float32)
    center = jnp.mean(values, axis=-1, keepdims=True)
    spread = jnp.mean(jnp.square(values - center), axis=-1, keepdims=True)
    normed = (values - center) * lax.rsqrt(spread + 1e-05) * gain[None, :] + shift[None, :]
    return jax.nn.silu(normed).astype(jnp.bfloat16)


def gate_rows(normed, w_value, w_gate):
    values = jnp.dot(normed, w_value, preferred_element_type=jnp.float32)
    gates = jnp.dot(normed, w_gate, preferred_element_type=jnp.float32)
    return (values * jax.nn.sigmoid(gates)).astype(jnp.bfloat16)


def per_device(
    stream,
    norm_gain,
    value_weight,
    gate_weight,
    conv_taps,
    conv_bias,
    channel_gain,
    channel_shift,
    out_weight,
):
    tokens = stream.shape[0]
    reach = conv_taps.shape[1] - 1
    hops = -(-reach // tokens)
    state = stream
    for layer in range(norm_gain.shape[0]):
        normed = rms_normed(state, norm_gain[layer])
        own_gated = gate_rows(normed, value_weight[layer], gate_weight[layer])
        pieces = [own_gated]
        for step in range(1, hops + 1):
            count = min(tokens, reach - (step - 1) * tokens)
            pieces.insert(0, passed_along(own_gated[tokens - count :], "sp", step))
        gated = jnp.concatenate(pieces, axis=0)
        conv = lax.conv_general_dilated(
            gated[None],
            conv_taps[layer][:, None, :],
            (1,),
            [(0, 0)],
            dimension_numbers=("NWC", "WIO", "NWC"),
            feature_group_count=gated.shape[1],
            preferred_element_type=jnp.float32,
        )[0]
        conv = (conv + conv_bias[layer][None, :]).astype(jnp.bfloat16)
        every_channel = lax.all_gather(conv, "tp", axis=1, tiled=True)
        mixed = channel_mix(every_channel, channel_gain[layer], channel_shift[layer])
        update = jnp.dot(mixed, out_weight[layer], preferred_element_type=jnp.float32)
        state = (state.astype(jnp.float32) + update).astype(jnp.bfloat16)
    return state


def solution(mesh):
    return jax.shard_map(
        per_device,
        mesh=mesh,
        in_specs=(
            P("sp", None),
            P(),
            P(None, None, "tp"),
            P(None, None, "tp"),
            P(None, None, "tp"),
            P(None, "tp"),
            P(),
            P(),
            P(),
        ),
        out_specs=P("sp", None),
        check_vma=False,
    )
```

profile of v0, /device:TPU:11, one launch (start us, length us, event | category | flops | bytes accessed | tf_op | source)
XLA Modules:
  0.0 94.5 jit_solution(958022671761127983)
XLA Ops:
  0.0 1.9 %fusion = f32[448]{0:T(512)S(1)} fusion(bf16[448,2048]{1,0:T(8,128)(2,1)} %param.9), kind=kLoop, calls=%fused_computation.6 | loop fusion | flops 2752064 | bytes 1836800 | tf_op jit(solution)/shard_map/reduce_sum | solution.py:15
  1.9 0.8 fusion.76
  2.8 0.0 copy-start
  2.8 0.0 copy-start.7
  2.8 2.6 %fusion.17 = f32[448,256]{1,0:T(8,128)S(1)} fusion(bf16[2,2048,256]{2,1,0:T(8,128)(2,1)} %param.12, bf16[448,2048]{1,0:T(8,128)(2,1)} %param.9, f32[2048]{0:T(1024)S(1)} %bitcast.46, f32[448]{0:T(512)S(1)} %add_rsqrt_fusion.3), kind=kOutput, calls=%fused_computation.27 | convolution fusion | flops 473776128 | bytes 3352320 | tf_op jit(solution)/shard_map/dot_general | solution.py:29
  5.4 0.0 copy-done
  5.4 0.3 copy-done.7
  5.8 0.0 copy-start.2
  5.8 0.0 copy-start.1
  5.8 0.0 copy-start.3
  5.8 0.0 copy-start.4
  5.8 0.7 fusion.18
  6.5 3.1 %collective-permute-start.1 = (bf16[448,256]{1,0:T(8,128)(2,1)S(1)}, bf16[448,256]{1,0:T(8,128)(2,1)S(1)}, u32[]{:S(2)}, u32[]{:S(2)}) collective-permute-start(bf16[448,256]{1,0:T(8,128)(2,1)S(1)} %fusion.18), channel_id=1, source_target_pairs={{0,2},{2,4},{4,6},{6,8},{8,10},{10,12},{12,14},{14,16},{16,18},{18... | collective-permute-start | bytes 688136 | tf_op jit(solution)/shard_map/ppermute | solution.py:10
  9.7 3.2 %collective-permute-start = (bf16[63,256]{1,0:T(8,128)(2,1)S(1)}, bf16[63,256]{1,0:T(8,128)(2,1)S(1)}, u32[]{:S(2)}, u32[]{:S(2)}) collective-permute-start(bf16[63,256]{1,0:T(8,128)(2,1)S(1)} %slice.72), channel_id=1, source_target_pairs={{0,4},{2,6},{4,8},{6,10},{8,12},{10,14},{12,16},{14,18},{16,20},{1... | collective-permute-start | bytes 96776 | tf_op jit(solution)/shard_map/ppermute | solution.py:10
  12.8 0.0 copy-done.2
  12.8 0.0 copy-done.1
  12.9 0.0 copy-done.3
  12.9 0.0 copy-done.4
  12.9 3.2 %collective-permute-done = bf16[63,256]{1,0:T(8,128)(2,1)S(1)} collective-permute-done((bf16[63,256]{1,0:T(8,128)(2,1)S(1)}, bf16[63,256]{1,0:T(8,128)(2,1)S(1)}, u32[]{:S(2)}, u32[]{:S(2)}) %collective-permute-start) | collective-permute-done | bytes 32288 | tf_op jit(solution)/shard_map/ppermute | solution.py:10
  16.2 0.0 collective-permute-done.1
  16.2 0.1 maximum_bitcast_fusion
  16.3 0.0 copy-start.5
  16.3 26.7 %fusion.34 = f32[1,448,256]{2,0,1:T(1,128)S(1)} fusion(bf16[1,959,256]{2,1,0:T(8,128)(2,1)S(1)} %maximum_bitcast_fusion, bf16[512,1,256]{2,0,1:T(8,128)(2,1)S(1)} %get-tuple-element.6), kind=kOutput, calls=%fused_computation.48 | convolution fusion | flops 117440512 | bytes 1211904 | tf_op jit(solution)/shard_map/conv_general_dilated | solution.py:56
  43.0 3.6 %all_gather.6 = bf16[448,512]{1,0:T(8,128)(2,1)S(1)} all-gather(bf16[448,256]{1,0:T(8,128)(2,1)S(1)} %fusion.63), channel_id=1, replica_groups=mesh['sp'=16,'tp'=2] {'tp'}, dimensions={1}, use_global_device_ids=true | all-gather | bytes 688128 | tf_op jit(solution)/shard_map/all_gather | solution.py:66
  46.6 0.1 convert_reduce_fusion.1
  46.8 0.3 fusion.45
  47.1 0.0 copy-done.5
  47.1 0.0 copy-start.6
  47.1 1.7 %fusion.4 = (f32[448]{0:T(512)S(1)}, bf16[448,2048]{1,0:T(8,128)(2,1)S(1)}) fusion(bf16[2,512,2048]{2,1,0:T(8,128)(2,1)S(1)} %copy-done.5, bf16[448,512]{1,0:T(8,128)(2,1)S(1)} %all_gather.6, f32[512]{0:T(512)S(1)} %bitcast.53, f32[512]{0:T(512)S(1)} %bitcast.52, f32[448]{0:T(512)S(1)} %add_rsqrt_fusion.2, f32[448]{0:T(512)S(1)} %broadcast_multiply_fusion.1, ...), kind=kOutput, calls=%fused_computation.10 | convolution fusion | flops 947322432 | bytes 6235904 | tf_op jit(solution)/shard_map/dot_general | solution.py:68
  48.8 0.0 copy-done.6
  48.8 0.7 fusion.14
  49.5 0.7 fusion.19
  50.2 3.2 %collective-permute-start.3 = (bf16[448,256]{1,0:T(8,128)(2,1)S(1)}, bf16[448,256]{1,0:T(8,128)(2,1)S(1)}, u32[]{:S(2)}, u32[]{:S(2)}) collective-permute-start(bf16[448,256]{1,0:T(8,128)(2,1)S(1)} %fusion.19), channel_id=1, source_target_pairs={{0,2},{2,4},{4,6},{6,8},{8,10},{10,12},{12,14},{14,16},{16,18},{18... | collective-permute-start | bytes 688136 | tf_op jit(solution)/shard_map/ppermute | solution.py:10
  53.4 4.0 %collective-permute-start.2 = (bf16[63,256]{1,0:T(8,128)(2,1)S(1)}, bf16[63,256]{1,0:T(8,128)(2,1)S(1)}, u32[]{:S(2)}, u32[]{:S(2)}) collective-permute-start(bf16[63,256]{1,0:T(8,128)(2,1)S(1)} %slice.73), channel_id=1, source_target_pairs={{0,4},{2,6},{4,8},{6,10},{8,12},{10,14},{12,16},{14,18},{16,20},{1... | collective-permute-start | bytes 96776 | tf_op jit(solution)/shard_map/ppermute | solution.py:10
  57.5 3.9 %collective-permute-done.2 = bf16[63,256]{1,0:T(8,128)(2,1)S(1)} collective-permute-done((bf16[63,256]{1,0:T(8,128)(2,1)S(1)}, bf16[63,256]{1,0:T(8,128)(2,1)S(1)}, u32[]{:S(2)}, u32[]{:S(2)}) %collective-permute-start.2) | collective-permute-done | bytes 32288 | tf_op jit(solution)/shard_map/ppermute | solution.py:10
  61.4 0.0 collective-permute-done.3
  61.4 0.1 maximum_bitcast_fusion.1
  61.5 26.6 %fusion.32 = f32[1,448,256]{2,0,1:T(1,128)S(1)} fusion(bf16[1,959,256]{2,1,0:T(8,128)(2,1)S(1)} %maximum_bitcast_fusion.1, bf16[512,1,256]{2,0,1:T(8,128)(2,1)S(1)} %get-tuple-element.5), kind=kOutput, calls=%fused_computation.46 | convolution fusion | flops 117440512 | bytes 1211904 | tf_op jit(solution)/shard_map/conv_general_dilated | solution.py:56
  88.2 3.3 %all_gather.7 = bf16[448,512]{1,0:T(8,128)(2,1)S(1)} all-gather(bf16[448,256]{1,0:T(8,128)(2,1)S(1)} %fusion.62), channel_id=1, replica_groups=mesh['sp'=16,'tp'=2] {'tp'}, dimensions={1}, use_global_device_ids=true | all-gather | bytes 688128 | tf_op jit(solution)/shard_map/all_gather | solution.py:66
  91.4 0.1 convert_reduce_fusion
  91.6 0.3 fusion.36
  91.9 2.6 %fusion.7 = bf16[448,2048]{1,0:T(8,128)(2,1)} fusion(bf16[448,2048]{1,0:T(8,128)(2,1)S(1)} %get-tuple-element.16, bf16[2,512,2048]{2,1,0:T(8,128)(2,1)S(1)} %copy-done.5, bf16[448,512]{1,0:T(8,128)(2,1)S(1)} %all_gather.7, f32[512]{0:T(512)S(1)} %bitcast.51, f32[512]{0:T(512)S(1)} %bitcast.50, f32[448]{0:T(512)S(1)} %add_rsqrt_fusion, ...), kind=kOutput, calls=%fused_computation.13 | convolution fusion | flops 944570368 | bytes 6234112 | tf_op jit(solution)/shard_map/dot_general | solution.py:68
  (14 shorter events, 0.2 us)
Async XLA Ops:
  2.8 2.7 %copy-start = (bf16[448,2048]{1,0:T(8,128)(2,1)S(1)}, bf16[448,2048]{1,0:T(8,128)(2,1)}, u32[]{:S(2)}) copy-start(bf16[448,2048]{1,0:T(8,128)(2,1)} %param.9) | copy-start | bytes 5505028
  2.8 3.0 %copy-start.7 = (bf16[2,2048,256]{2,1,0:T(8,128)(2,1)S(1)}, bf16[2,2048,256]{2,1,0:T(8,128)(2,1)}, u32[]{:S(2)}) copy-start(bf16[2,2048,256]{2,1,0:T(8,128)(2,1)} %param.11) | copy-start | bytes 6291460
  5.8 7.0 %copy-start.2 = (f32[2,512]{1,0:T(2,128)S(1)}, f32[2,512]{1,0:T(2,128)}, u32[]{:S(2)}) copy-start(f32[2,512]{1,0:T(2,128)} %param.15) | copy-start | bytes 12292
  5.8 7.1 %copy-start.1 = (bf16[2,512,256]{2,1,0:T(8,128)(2,1)S(1)}, bf16[2,512,256]{2,1,0:T(8,128)(2,1)}, u32[]{:S(2)}) copy-start(bf16[2,512,256]{2,1,0:T(8,128)(2,1)} %param.13) | copy-start | bytes 1572868
  5.8 7.1 %copy-start.3 = (f32[2,512]{1,0:T(2,128)S(1)}, f32[2,512]{1,0:T(2,128)}, u32[]{:S(2)}) copy-start(f32[2,512]{1,0:T(2,128)} %param.16) | copy-start | bytes 12292
  5.8 7.1 %copy-start.4 = (f32[2,256]{1,0:T(2,128)S(1)}, f32[2,256]{1,0:T(2,128)}, u32[]{:S(2)}) copy-start(f32[2,256]{1,0:T(2,128)} %param.14) | copy-start | bytes 6148
  6.5 9.7 %collective-permute-start.1 = (bf16[448,256]{1,0:T(8,128)(2,1)S(1)}, bf16[448,256]{1,0:T(8,128)(2,1)S(1)}, u32[]{:S(2)}, u32[]{:S(2)}) collective-permute-start(bf16[448,256]{1,0:T(8,128)(2,1)S(1)} %fusion.18), channel_id=1, source_target_pairs={{0,2},{2,4},{4,6},{6,8},{8,10},{10,12},{12,14},{14,16},{16,18},{18... | collective-permute-start | bytes 688136 | tf_op jit(solution)/shard_map/ppermute | solution.py:10
  9.7 6.5 %collective-permute-start = (bf16[63,256]{1,0:T(8,128)(2,1)S(1)}, bf16[63,256]{1,0:T(8,128)(2,1)S(1)}, u32[]{:S(2)}, u32[]{:S(2)}) collective-permute-start(bf16[63,256]{1,0:T(8,128)(2,1)S(1)} %slice.72), channel_id=1, source_target_pairs={{0,4},{2,6},{4,8},{6,10},{8,12},{10,14},{12,16},{14,18},{16,20},{1... | collective-permute-start | bytes 96776 | tf_op jit(solution)/shard_map/ppermute | solution.py:10
  16.3 30.8 %copy-start.5 = (bf16[2,512,2048]{2,1,0:T(8,128)(2,1)S(1)}, bf16[2,512,2048]{2,1,0:T(8,128)(2,1)}, u32[]{:S(2)}) copy-start(bf16[2,512,2048]{2,1,0:T(8,128)(2,1)} %param.17) | copy-start | bytes 12582916
  47.1 1.7 %copy-start.6 = (bf16[2,2048,256]{2,1,0:T(8,128)(2,1)S(1)}, bf16[2,2048,256]{2,1,0:T(8,128)(2,1)}, u32[]{:S(2)}) copy-start(bf16[2,2048,256]{2,1,0:T(8,128)(2,1)} %param.12) | copy-start | bytes 6291460
  50.2 11.1 %collective-permute-start.3 = (bf16[448,256]{1,0:T(8,128)(2,1)S(1)}, bf16[448,256]{1,0:T(8,128)(2,1)S(1)}, u32[]{:S(2)}, u32[]{:S(2)}) collective-permute-start(bf16[448,256]{1,0:T(8,128)(2,1)S(1)} %fusion.19), channel_id=1, source_target_pairs={{0,2},{2,4},{4,6},{6,8},{8,10},{10,12},{12,14},{14,16},{16,18},{18... | collective-permute-start | bytes 688136 | tf_op jit(solution)/shard_map/ppermute | solution.py:10
  53.4 7.9 %collective-permute-start.2 = (bf16[63,256]{1,0:T(8,128)(2,1)S(1)}, bf16[63,256]{1,0:T(8,128)(2,1)S(1)}, u32[]{:S(2)}, u32[]{:S(2)}) collective-permute-start(bf16[63,256]{1,0:T(8,128)(2,1)S(1)} %slice.73), channel_id=1, source_target_pairs={{0,4},{2,6},{4,8},{6,10},{8,12},{10,14},{12,16},{14,18},{16,20},{1... | collective-permute-start | bytes 96776 | tf_op jit(solution)/shard_map/ppermute | solution.py:10
where the time goes:
time: 95.7 us; the launch traced here: 94.5 us
  matrix products  62.4 us (65%)
  starting transfers between devices  13.5 us (14%)
  waiting for transfers between devices  7.12 us (7%)
  blocking collectives  6.88 us (7%)
  other arithmetic  3.19 us (3%)
  local copies, waits for them, and re-layouts  1.27 us (1%)
    conv_general_dilated x2, matrix products, per_device(): lax.conv_general_dilated(gated[None], conv_taps[layer][:, None, :], (1,),...  53.3 us
    ppermute x4, starting transfers between devices, passed_along(): return lax.ppermute(value, axis, pairs)  13.5 us
    ppermute x4, waiting for transfers between devices, passed_along(): return lax.ppermute(value, axis, pairs)  7.12 us
    all_gather x2, blocking collectives, per_device(): every_channel = lax.all_gather(conv, 'tp', axis=1, tiled=True)  6.88 us
    dot_general x2, matrix products, per_device(): jnp.dot(mixed, out_weight[layer], preferred_element_type=jnp.float32)  4.28 us
    dot_general x2, matrix products, gate_rows(): gates = jnp.dot(normed, w_gate, preferred_element_type=jnp.float32)  3.35 us
    reduce_sum x1, other arithmetic, rms_normed(): scale = lax.rsqrt(jnp.mean(values * values, axis=-1, keepdims=True) + 1e-06)  1.94 us
  transfers between devices with their start and end apart: 4, of which 2 were waited for; matrix products, arithmetic and copies ran while one was open for 0% of the time, Pallas kernels for 0%

commit v1 on v0

--- a/solution.py
+++ b/solution.py
@@ -1,4 +1,5 @@
 import jax
+import numpy as np
 import jax.numpy as jnp
 from jax import lax
 from jax.sharding import PartitionSpec as P
@@ -30,6 +31,45 @@
     return (values * jax.nn.sigmoid(gates)).astype(jnp.bfloat16)
 
 
+BLOCK = 128
+
+
+def dft_matrices(block):
+    span = 2 * block
+    angle = 2 * np.pi / span * np.outer(np.arange(block) + 0.5, np.arange(span))
+    forward = np.concatenate([np.cos(angle), -np.sin(angle)], axis=0)
+    of_taps = forward[:, block - 1 :: -1]
+    inverse = forward[:, block:].T / block
+    return [jnp.asarray(m, jnp.bfloat16) for m in (forward, of_taps, inverse)]
+
+
+def long_conv(gated, taps, tokens):
+    forward, of_taps, inverse = dft_matrices(BLOCK)
+    parts = taps.shape[0] // BLOCK
+    outs = -(-tokens // BLOCK)
+    rows = (parts + outs) * BLOCK
+    gated = jnp.pad(gated, ((rows - gated.shape[0], 0), (0, 0)))
+    spectra = []
+    for w in range(parts + outs - 1):
+        window = gated[w * BLOCK : (w + 2) * BLOCK]
+        spectra.append(jnp.dot(forward, window, preferred_element_type=jnp.float32))
+    kernels = []
+    for j in range(parts):
+        part = taps[(parts - 1 - j) * BLOCK : (parts - j) * BLOCK]
+        kernels.append(jnp.dot(of_taps, part, preferred_element_type=jnp.float32))
+    results = []
+    for p in range(outs):
+        real = imag = 0.0
+        for j in range(parts):
+            x, h = spectra[parts - 1 + p - j], kernels[j]
+            xr, xi, hr, hi = x[:BLOCK], x[BLOCK:], h[:BLOCK], h[BLOCK:]
+            real = real + xr * hr - xi * hi
+            imag = imag + xr * hi + xi * hr
+        both = jnp.concatenate([real, imag], axis=0).astype(jnp.bfloat16)
+        results.append(jnp.dot(inverse, both, preferred_element_type=jnp.float32))
+    return jnp.concatenate(results, axis=0)[outs * BLOCK - tokens :]
+
+
 def per_device(
     stream,
     norm_gain,
@@ -53,15 +93,7 @@
             count = min(tokens, reach - (step - 1) * tokens)
             pieces.insert(0, passed_along(own_gated[tokens - count :], "sp", step))
         gated = jnp.concatenate(pieces, axis=0)
-        conv = lax.conv_general_dilated(
-            gated[None],
-            conv_taps[layer][:, None, :],
-            (1,),
-            [(0, 0)],
-            dimension_numbers=("NWC", "WIO", "NWC"),
-            feature_group_count=gated.shape[1],
-            preferred_element_type=jnp.float32,
-        )[0]
+        conv = long_conv(gated, conv_taps[layer], tokens)
         conv = (conv + conv_bias[layer][None, :]).astype(jnp.bfloat16)
         every_channel = lax.all_gather(conv, "tp", axis=1, tiled=True)
         mixed = channel_mix(every_channel, channel_gain[layer], channel_shift[layer])

time: 95.7 us -> 48.1 us (0.50)
  the two profiles are of different devices: /device:TPU:11 before, /device:TPU:25 now
where the time goes in v1:
time: 48.1 us; the launch traced here: 47.7 us
  matrix products  16.5 us (34%)
  starting transfers between devices  10.2 us (21%)
  waiting for transfers between devices  8.98 us (19%)
  blocking collectives  7.16 us (15%)
  other arithmetic  2.96 us (6%)
  local copies, waits for them, and re-layouts  1.26 us (3%)
  between operations  0.6 us (1%)
    ppermute x4, starting transfers between devices, passed_along(): return lax.ppermute(value, axis, pairs)  10.2 us
    ppermute x4, waiting for transfers between devices, passed_along(): return lax.ppermute(value, axis, pairs)  8.98 us
    all_gather x2, blocking collectives, per_device(): every_channel = lax.all_gather(conv, 'tp', axis=1, tiled=True)  7.16 us
    dot_general x2, matrix products, per_device(): jnp.dot(mixed, out_weight[layer], preferred_element_type=jnp.float32)  4.29 us
    dot_general x16, matrix products, long_conv(): results.append(jnp.dot(inverse, both, preferred_element_type=jnp.float32))  3.59 us
    dot_general x2, matrix products, gate_rows(): gates = jnp.dot(normed, w_gate, preferred_element_type=jnp.float32)  3.36 us
    dot_general x14, matrix products, long_conv(): spectra.append(jnp.dot(forward, window, preferred_element_type=jnp.float32))  2.55 us
    reduce_sum x1, other arithmetic, rms_normed(): scale = lax.rsqrt(jnp.mean(values * values, axis=-1, keepdims=True) + 1e-06)  1.94 us
  transfers between devices with their start and end apart: 4, of which 2 were waited for; matrix products, arithmetic and copies ran while one was open for 7% of the time, Pallas kernels for 0%

profile of v1, /device:TPU:25, one launch (start us, length us, event | category | flops | bytes accessed | tf_op | source)
XLA Modules:
  0.0 47.7 jit_solution(2617931705711893870)
XLA Ops:
  0.0 0.8 %fusion.182 = (f32[1,2048]{1,0:T(1,128)S(1)}, f32[1,2048]{1,0:T(1,128)S(1)}) fusion(f32[2,2048]{1,0:T(2,128)} %param.16), kind=kLoop, calls=%fused_computation.223 | loop fusion | bytes 32768 | tf_op jit(solution)/shard_map/slice | solution.py:89
  0.8 1.9 %fusion = f32[448]{0:T(512)S(1)} fusion(bf16[448,2048]{1,0:T(8,128)(2,1)} %param.15), kind=kLoop, calls=%fused_computation.6 | loop fusion | flops 2752064 | bytes 1836800 | tf_op jit(solution)/shard_map/reduce_sum | solution.py:16
  2.8 2.6 %fusion.17 = f32[448,256]{1,0:T(8,128)S(1)} fusion(bf16[2,2048,256]{2,1,0:T(8,128)(2,1)} %param.18, bf16[448,2048]{1,0:T(8,128)(2,1)} %param.15, f32[2048]{0:T(1024)S(1)} %bitcast.108, f32[448]{0:T(512)S(1)} %add_rsqrt_fusion.3), kind=kOutput, calls=%fused_computation.27 | convolution fusion | flops 473776128 | bytes 3352320 | tf_op jit(solution)/shard_map/dot_general | solution.py:30
  5.4 0.3 copy-done.11
  5.8 0.7 %fusion.18 = bf16[448,256]{1,0:T(8,128)(2,1)S(1)} fusion(f32[448,256]{1,0:T(8,128)S(1)} %fusion.17, bf16[2,2048,256]{2,1,0:T(8,128)(2,1)S(1)} %copy-done.11, bf16[448,2048]{1,0:T(8,128)(2,1)S(1)} %copy-done.4, f32[2048]{0:T(1024)S(1)} %bitcast.109, f32[448]{0:T(512)S(1)} %add_rsqrt_fusion.3), kind=kOutput, calls=%fused_computation.28 | convolution fusion | flops 473661440 | bytes 3581952 | tf_op jit(solution)/shard_map/dot_general | solution.py:29
  6.5 3.3 %collective-permute-start = (bf16[448,256]{1,0:T(8,128)(2,1)S(1)}, bf16[448,256]{1,0:T(8,128)(2,1)S(1)}, u32[]{:S(2)}, u32[]{:S(2)}) collective-permute-start(bf16[448,256]{1,0:T(8,128)(2,1)S(1)} %fusion.18), channel_id=1, source_target_pairs={{0,2},{2,4},{4,6},{6,8},{8,10},{10,12},{12,14},{14,16},{16,18},{18... | collective-permute-start | bytes 688136 | tf_op jit(solution)/shard_map/ppermute | solution.py:11
  9.8 3.1 %collective-permute-start.1 = (bf16[63,256]{1,0:T(8,128)(2,1)S(1)}, bf16[63,256]{1,0:T(8,128)(2,1)S(1)}, u32[]{:S(2)}, u32[]{:S(2)}) collective-permute-start(bf16[63,256]{1,0:T(8,128)(2,1)S(1)} %slice.516), channel_id=1, source_target_pairs={{0,4},{2,6},{4,8},{6,10},{8,12},{10,14},{12,16},{14,18},{16,20},{1... | collective-permute-start | bytes 96776 | tf_op jit(solution)/shard_map/ppermute | solution.py:11
  13.7 0.2 fusion.115
  13.9 0.2 fusion.113
  14.8 2.3 %collective-permute-done = bf16[448,256]{1,0:T(8,128)(2,1)S(1)} collective-permute-done((bf16[448,256]{1,0:T(8,128)(2,1)S(1)}, bf16[448,256]{1,0:T(8,128)(2,1)S(1)}, u32[]{:S(2)}, u32[]{:S(2)}) %collective-permute-start) | collective-permute-done | bytes 229408 | tf_op jit(solution)/shard_map/ppermute | solution.py:11
  17.2 0.2 fusion.128
  17.4 0.2 fusion.126
  17.5 0.2 fusion.130
  17.8 0.2 fusion.86
  18.0 0.2 fusion.160
  18.2 0.2 fusion.117
  18.4 0.2 fusion.161
  18.6 0.2 fusion.27
  18.9 0.2 fusion.26
  19.1 0.2 fusion.162
  19.3 0.2 fusion.25
  19.6 0.2 fusion.163
  19.8 0.2 fusion.24
  20.1 3.8 %all_gather.6 = bf16[448,512]{1,0:T(8,128)(2,1)S(1)} all-gather(bf16[448,256]{1,0:T(8,128)(2,1)S(1)} %fusion.67), channel_id=1, replica_groups=mesh['sp'=16,'tp'=2] {'tp'}, dimensions={1}, use_global_device_ids=true | all-gather | bytes 688128 | tf_op jit(solution)/shard_map/all_gather | solution.py:98
  24.0 0.3 fusion.49
  24.4 1.7 %fusion.4 = (f32[448]{0:T(512)S(1)}, bf16[448,2048]{1,0:T(8,128)(2,1)S(1)}) fusion(bf16[2,512,2048]{2,1,0:T(8,128)(2,1)S(1)} %copy-done.9, bf16[448,512]{1,0:T(8,128)(2,1)S(1)} %all_gather.6, f32[512]{0:T(512)S(1)} %bitcast.115, f32[512]{0:T(512)S(1)} %bitcast.114, f32[448]{0:T(512)S(1)} %add_rsqrt_fusion.2, f32[448]{0:T(512)S(1)} %broadcast_multiply_fusion.1, ...), kind=kOutput, calls=%fused_computation.10 | convolution fusion | flops 947322432 | bytes 6235904 | tf_op jit(solution)/shard_map/dot_general | solution.py:100
  26.1 0.7 %fusion.14 = f32[448,256]{1,0:T(8,128)S(1)} fusion(bf16[2,2048,256]{2,1,0:T(8,128)(2,1)S(1)} %copy-done.10, bf16[448,2048]{1,0:T(8,128)(2,1)S(1)} %get-tuple-element.14, f32[2048]{0:T(1024)S(1)} %bitcast.106, f32[448]{0:T(512)S(1)} %add_rsqrt_fusion.1), kind=kOutput, calls=%fused_computation.23 | convolution fusion | flops 473776128 | bytes 3352576 | tf_op jit(solution)/shard_map/dot_general | solution.py:30
  26.8 0.7 %fusion.19 = bf16[448,256]{1,0:T(8,128)(2,1)S(1)} fusion(f32[448,256]{1,0:T(8,128)S(1)} %fusion.14, bf16[2,2048,256]{2,1,0:T(8,128)(2,1)S(1)} %copy-done.11, bf16[448,2048]{1,0:T(8,128)(2,1)S(1)} %get-tuple-element.14, f32[2048]{0:T(1024)S(1)} %bitcast.107, f32[448]{0:T(512)S(1)} %add_rsqrt_fusion.1), kind=kOutput, calls=%fused_computation.29 | convolution fusion | flops 473661440 | bytes 3581952 | tf_op jit(solution)/shard_map/dot_general | solution.py:29
  27.5 1.9 %collective-permute-start.2 = (bf16[448,256]{1,0:T(8,128)(2,1)S(1)}, bf16[448,256]{1,0:T(8,128)(2,1)S(1)}, u32[]{:S(2)}, u32[]{:S(2)}) collective-permute-start(bf16[448,256]{1,0:T(8,128)(2,1)S(1)} %fusion.19), channel_id=1, source_target_pairs={{0,2},{2,4},{4,6},{6,8},{8,10},{10,12},{12,14},{14,16},{16,18},{18... | collective-permute-start | bytes 688136 | tf_op jit(solution)/shard_map/ppermute | solution.py:11
  29.4 0.2 fusion.98
  29.6 1.9 %collective-permute-start.3 = (bf16[63,256]{1,0:T(8,128)(2,1)S(1)}, bf16[63,256]{1,0:T(8,128)(2,1)S(1)}, u32[]{:S(2)}, u32[]{:S(2)}) collective-permute-start(bf16[63,256]{1,0:T(8,128)(2,1)S(1)} %slice.543), channel_id=1, source_target_pairs={{0,4},{2,6},{4,8},{6,10},{8,12},{10,14},{12,16},{14,18},{16,20},{1... | collective-permute-start | bytes 96776 | tf_op jit(solution)/shard_map/ppermute | solution.py:11
  31.6 0.2 fusion.96
  31.7 6.7 %collective-permute-done.2 = bf16[448,256]{1,0:T(8,128)(2,1)S(1)} collective-permute-done((bf16[448,256]{1,0:T(8,128)(2,1)S(1)}, bf16[448,256]{1,0:T(8,128)(2,1)S(1)}, u32[]{:S(2)}, u32[]{:S(2)}) %collective-permute-start.2) | collective-permute-done | bytes 229408 | tf_op jit(solution)/shard_map/ppermute | solution.py:11
  38.6 0.2 fusion.107
  38.8 0.2 fusion.109
  39.0 0.2 fusion.92
  39.2 0.2 fusion.164
  39.4 0.2 fusion.23
  39.6 0.2 fusion.100
  39.8 0.2 fusion.165
  40.0 0.2 fusion.22
  40.3 0.2 fusion.166
  40.5 0.2 fusion.21
  40.8 0.2 fusion.167
  41.0 0.2 fusion.20
  41.3 3.4 %all_gather.7 = bf16[448,512]{1,0:T(8,128)(2,1)S(1)} all-gather(bf16[448,256]{1,0:T(8,128)(2,1)S(1)} %fusion.65), channel_id=1, replica_groups=mesh['sp'=16,'tp'=2] {'tp'}, dimensions={1}, use_global_device_ids=true | all-gather | bytes 688128 | tf_op jit(solution)/shard_map/all_gather | solution.py:98
  44.8 0.3 fusion.40
  45.1 2.6 %fusion.7 = bf16[448,2048]{1,0:T(8,128)(2,1)} fusion(bf16[448,2048]{1,0:T(8,128)(2,1)S(1)} %get-tuple-element.14, bf16[2,512,2048]{2,1,0:T(8,128)(2,1)S(1)} %copy-done.9, bf16[448,512]{1,0:T(8,128)(2,1)S(1)} %all_gather.7, f32[512]{0:T(512)S(1)} %bitcast.113, f32[512]{0:T(512)S(1)} %bitcast.112, f32[448]{0:T(512)S(1)} %add_rsqrt_fusion, ...), kind=kOutput, calls=%fused_computation.13 | convolution fusion | flops 944570368 | bytes 6234112 | tf_op jit(solution)/shard_map/dot_general | solution.py:100
  (49 shorter events, 2.0 us)
Async XLA Ops:
  2.8 2.7 %copy-start.4 = (bf16[448,2048]{1,0:T(8,128)(2,1)S(1)}, bf16[448,2048]{1,0:T(8,128)(2,1)}, u32[]{:S(2)}) copy-start(bf16[448,2048]{1,0:T(8,128)(2,1)} %param.15) | copy-start | bytes 5505028
  2.8 3.0 %copy-start.11 = (bf16[2,2048,256]{2,1,0:T(8,128)(2,1)S(1)}, bf16[2,2048,256]{2,1,0:T(8,128)(2,1)}, u32[]{:S(2)}) copy-start(bf16[2,2048,256]{2,1,0:T(8,128)(2,1)} %param.17) | copy-start | bytes 6291460
  5.8 7.2 %copy-start.1 = (bf16[256,128]{1,0:T(8,128)(2,1)S(1)}, bf16[256,128]{1,0:T(8,128)(2,1)}, u32[]{:S(2)}) copy-start(bf16[256,128]{1,0:T(8,128)(2,1)} %constant.31.clone) | copy-start | bytes 196612
  5.8 7.2 %copy-start.5 = (bf16[2,512,256]{2,1,0:T(8,128)(2,1)S(1)}, bf16[2,512,256]{2,1,0:T(8,128)(2,1)}, u32[]{:S(2)}) copy-start(bf16[2,512,256]{2,1,0:T(8,128)(2,1)} %param.19) | copy-start | bytes 1572868
  5.8 7.9 %copy-start = (bf16[256,256]{1,0:T(8,128)(2,1)S(1)}, bf16[256,256]{1,0:T(8,128)(2,1)}, u32[]{:S(2)}) copy-start(bf16[256,256]{1,0:T(8,128)(2,1)} %constant.30.clone) | copy-start | bytes 393220
  6.5 8.1 %copy-start.8 = (f32[2,256]{1,0:T(2,128)S(1)}, f32[2,256]{1,0:T(2,128)}, u32[]{:S(2)}) copy-start(f32[2,256]{1,0:T(2,128)} %param.20) | copy-start | bytes 6148
  6.5 8.1 %copy-start.6 = (f32[2,512]{1,0:T(2,128)S(1)}, f32[2,512]{1,0:T(2,128)}, u32[]{:S(2)}) copy-start(f32[2,512]{1,0:T(2,128)} %param.21) | copy-start | bytes 12292
  6.5 8.1 %copy-start.7 = (f32[2,512]{1,0:T(2,128)S(1)}, f32[2,512]{1,0:T(2,128)}, u32[]{:S(2)}) copy-start(f32[2,512]{1,0:T(2,128)} %param.22) | copy-start | bytes 12292
  6.5 10.6 %collective-permute-start = (bf16[448,256]{1,0:T(8,128)(2,1)S(1)}, bf16[448,256]{1,0:T(8,128)(2,1)S(1)}, u32[]{:S(2)}, u32[]{:S(2)}) collective-permute-start(bf16[448,256]{1,0:T(8,128)(2,1)S(1)} %fusion.18), channel_id=1, source_target_pairs={{0,2},{2,4},{4,6},{6,8},{8,10},{10,12},{12,14},{14,16},{16,18},{18... | collective-permute-start | bytes 688136 | tf_op jit(solution)/shard_map/ppermute | solution.py:11
  9.8 7.9 %collective-permute-start.1 = (bf16[63,256]{1,0:T(8,128)(2,1)S(1)}, bf16[63,256]{1,0:T(8,128)(2,1)S(1)}, u32[]{:S(2)}, u32[]{:S(2)}) collective-permute-start(bf16[63,256]{1,0:T(8,128)(2,1)S(1)} %slice.516), channel_id=1, source_target_pairs={{0,4},{2,6},{4,8},{6,10},{8,12},{10,14},{12,16},{14,18},{16,20},{1... | collective-permute-start | bytes 96776 | tf_op jit(solution)/shard_map/ppermute | solution.py:11
  14.2 3.7 %copy-start.2 = (bf16[128,128]{1,0:T(8,128)(2,1)S(1)}, bf16[128,128]{1,0:T(8,128)(2,1)}, u32[]{:S(2)}) copy-start(bf16[128,128]{1,0:T(8,128)(2,1)} %constant.37) | copy-start | bytes 98308
  17.7 0.9 %copy-start.3 = (bf16[128,128]{1,0:T(8,128)(2,1)S(1)}, bf16[128,128]{1,0:T(8,128)(2,1)}, u32[]{:S(2)}) copy-start(bf16[128,128]{1,0:T(8,128)(2,1)} %constant.38) | copy-start | bytes 98308
  19.6 4.8 %copy-start.9 = (bf16[2,512,2048]{2,1,0:T(8,128)(2,1)S(1)}, bf16[2,512,2048]{2,1,0:T(8,128)(2,1)}, u32[]{:S(2)}) copy-start(bf16[2,512,2048]{2,1,0:T(8,128)(2,1)} %param.23) | copy-start | bytes 12582916
  24.4 1.7 %copy-start.10 = (bf16[2,2048,256]{2,1,0:T(8,128)(2,1)S(1)}, bf16[2,2048,256]{2,1,0:T(8,128)(2,1)}, u32[]{:S(2)}) copy-start(bf16[2,2048,256]{2,1,0:T(8,128)(2,1)} %param.18) | copy-start | bytes 6291460
  27.5 10.9 %collective-permute-start.2 = (bf16[448,256]{1,0:T(8,128)(2,1)S(1)}, bf16[448,256]{1,0:T(8,128)(2,1)S(1)}, u32[]{:S(2)}, u32[]{:S(2)}) collective-permute-start(bf16[448,256]{1,0:T(8,128)(2,1)S(1)} %fusion.19), channel_id=1, source_target_pairs={{0,2},{2,4},{4,6},{6,8},{8,10},{10,12},{12,14},{14,16},{16,18},{18... | collective-permute-start | bytes 688136 | tf_op jit(solution)/shard_map/ppermute | solution.py:11
  29.6 9.3 %collective-permute-start.3 = (bf16[63,256]{1,0:T(8,128)(2,1)S(1)}, bf16[63,256]{1,0:T(8,128)(2,1)S(1)}, u32[]{:S(2)}, u32[]{:S(2)}) collective-permute-start(bf16[63,256]{1,0:T(8,128)(2,1)S(1)} %slice.543), channel_id=1, source_target_pairs={{0,4},{2,6},{4,8},{6,10},{8,12},{10,14},{12,16},{14,18},{16,20},{1... | collective-permute-start | bytes 96776 | tf_op jit(solution)/shard_map/ppermute | solution.py:11
